TPU v7x, 32 devices: a whole 2x2x4 slice. The times are simulated.
32 devices in a mesh: fs: 8 (over z, y), tp: 4 (over x, core).
Axes of the slice: x: 2, y: 2, z: 4, core: 2. Of those that a mesh axis runs over, the one named last changes fastest.
Arguments:
- later_input: bfloat16 [4096, 2048], P(('fs', 'tp')), may hold values from -6 to 6
- earlier_input: bfloat16 [4096, 2048], P('fs'), may hold values from -6 to 6
- earlier_hidden: bfloat16 [4096, 4096], P('fs', 'tp'), may hold values from -6 to 6
- cotangent: bfloat16 [4096, 2048], P('fs'), may hold values from -6 to 6
- up_weight: bfloat16 [2048, 4096], P('fs', 'tp'), may hold values from -0.125 to 0.125
- down_weight: bfloat16 [4096, 2048], P(('tp', 'fs')), may hold values from -0.09375 to 0.09375
- up_sum: float32 [2048, 4096], P('fs', 'tp'), may hold values from -4 to 4
- down_sum: float32 [4096, 2048], P(('tp', 'fs')), may hold values from -4 to 4
Outputs:
- later_output: bfloat16 [4096, 2048], P(('fs', 'tp'))
- later_hidden: bfloat16 [4096, 4096], P('fs', 'tp')
- earlier_grad: bfloat16 [4096, 2048], P(('fs', 'tp'))
- up_sum_next: float32 [2048, 4096], P('fs', 'tp')
- down_sum_next: float32 [4096, 2048], P(('tp', 'fs'))
All inputs are finite; a program needn't handle non-finite values.
Results may differ from a plain program's by a relative error of at most 0.0095.
Values may be sent and summed in bfloat16 or wider, within the bound.
A program may use at most 128 MiB of HBM per device.

v0:
```python
import jax
import jax.numpy as jnp
from jax import lax
from jax.sharding import PartitionSpec as P


def contract_last(left_rows, right_rows):
    return lax.dot_general(
        left_rows, right_rows, (((1,), (1,)), ((), ())), preferred_element_type=jnp.float32
    )


def contract_first(left_rows, right_rows):
    return lax.dot_general(
        left_rows, right_rows, (((0,), (0,)), ((), ())), preferred_element_type=jnp.float32
    )


def shards(
    later_input, earlier_input, earlier_hidden, cotangent, up_weight, down_weight, up_sum, down_sum
):
    gathered = lax.all_gather(later_input, "tp", axis=0, tiled=True)
    groups = lax.axis_size("fs")
    grad_scale = float(earlier_input.shape[0] * groups) ** (-0.5)
    lifted = jnp.maximum(earlier_hidden.astype(jnp.float32), 0.0)
    activation = (lifted * lifted).astype(jnp.bfloat16)
    up_front, down_front = (
        lax.all_gather(up_weight, "fs", axis=0, tiled=True),
        lax.all_gather(down_weight, "fs", axis=0, tiled=True),
    )
    later_hidden = jnp.dot(gathered, up_front, preferred_element_type=jnp.float32).astype(
        jnp.bfloat16
    )
    lifted_later = jnp.maximum(later_hidden.astype(jnp.float32), 0.0)
    act_later = (lifted_later * lifted_later).astype(jnp.bfloat16)
    rows_here = act_later
    later_output = lax.psum_scatter(
        jnp.dot(rows_here, down_front, preferred_element_type=jnp.float32).astype(jnp.bfloat16),
        "tp",
        scatter_dimension=0,
        tiled=True,
    )
    up_back, down_back = (up_front, down_front)
    act_slope = contract_last(cotangent, down_back)
    pre_grad = (2.0 * act_slope * lifted).astype(jnp.bfloat16)
    rows_here = pre_grad
    earlier_grad = lax.psum_scatter(
        contract_last(rows_here, up_back).astype(jnp.bfloat16),
        "tp",
        scatter_dimension=0,
        tiled=True,
    )
    columns = earlier_input
    up_total = lax.psum_scatter(
        contract_first(columns, pre_grad), "fs", scatter_dimension=0, tiled=True
    )
    earlier_grad, up_total = (earlier_grad, up_total)
    columns = activation
    down_total = lax.psum_scatter(
        contract_first(columns, cotangent), "fs", scatter_dimension=0, tiled=True
    )
    return (
        later_output,
        later_hidden,
        earlier_grad,
        up_sum + grad_scale * up_total,
        down_sum + grad_scale * down_total,
    )


def solution(mesh):
    in_specs = (
        P(("fs", "tp"), None),
        P("fs", None),
        P("fs", "tp"),
        P("fs", None),
        P("fs", "tp"),
        P(("tp", "fs"), None),
        P("fs", "tp"),
        P(("tp", "fs"), None),
    )
    out_specs = (
        P(("fs", "tp"), None),
        P("fs", "tp"),
        P(("fs", "tp"), None),
        P("fs", "tp"),
        P(("tp", "fs"), None),
    )
    return jax.shard_map(shards, mesh=mesh, in_specs=in_specs, out_specs=out_specs, check_vma=False)
```

profile of v0, /device:TPU:0, one launch (start us, length us, event | category | flops | bytes accessed | tf_op | source)
XLA Modules:
  0.0 557.7 jit_solution(5843369301261905202)
XLA Ops:
  7.2 0.0 copy-start
  7.2 0.0 all-gather.8.cloned.1.call-start
  7.2 0.7 all-gather.8.cloned.1.call-update
  7.9 0.0 all-gather.6.cloned.1.call-start
  8.0 0.7 all-gather.6.cloned.1.call-update
  8.7 0.0 all-gather.4.cloned.1.call-start
  8.7 0.7 all-gather.4.cloned.1.call-update
  9.4 0.0 reduce-scatter.11.cloned.1.call-start
  9.4 0.0 copy-done
  9.5 6.9 %fusion = f32[1024,2048]{1,0:T(8,128)} fusion(bf16[512,2048]{1,0:T(8,128)(2,1)S(1)} %copy-done, bf16[512,1024]{1,0:T(8,128)(2,1)} %param.10), kind=kOutput, calls=%fused_computation.8 | convolution fusion | flops 2149580800 | bytes 11534336 | tf_op jit(solution)/shard_map/dot_general | solution.py:14
  16.3 0.0 copy-start.3
  16.3 0.0 reduce-scatter.11.cloned.1.call-update
  16.3 0.0 reduce-scatter.9.cloned.1.call-start
  16.4 69.3 %all-gather.8.cloned.1.call-done = bf16[1024,2048]{1,0:T(8,128)(2,1)} async-done(((bf16[128,2048]{1,0:T(8,128)(2,1)}), bf16[1024,2048]{1,0:T(8,128)(2,1)}) %all-gather.8.cloned.1.call-update) | async-done | bytes 4194320 | tf_op jit(solution)/shard_map/all_gather | solution.py:29
  85.7 0.0 copy-done.3
  85.7 0.0 copy-start.2
  85.7 4.7 multiply_convert_fusion.1
  90.4 0.0 copy-start.5
  90.4 1.0 copy-done.5
  91.4 0.0 copy-done.2
  91.4 5.6 %convolution_bitcast_fusion = f32[2048,1024]{0,1:T(8,128)} fusion(bf16[512,1024]{1,0:T(8,128)(2,1)S(1)} %multiply_convert_fusion.1, bf16[512,2048]{1,0:T(8,128)(2,1)S(1)} %copy-done.2), kind=kOutput, calls=%fused_computation | convolution fusion | flops 2147483648 | bytes 11534336 | tf_op jit(solution)/shard_map/dot_general | solution.py:14
  97.0 0.0 copy-start.6
  97.0 0.0 reduce-scatter.9.cloned.1.call-update
  97.0 0.0 reduce-scatter.7.cloned.1.call-start
  97.1 62.1 %all-gather.6.cloned.1.call-done = bf16[2048,1024]{1,0:T(8,128)(2,1)} async-done(((bf16[256,1024]{1,0:T(8,128)(2,1)}), bf16[2048,1024]{1,0:T(8,128)(2,1)}) %all-gather.6.cloned.1.call-update) | async-done | bytes 4194320 | tf_op jit(solution)/shard_map/all_gather | solution.py:28
  159.1 0.0 copy-done.6
  159.1 5.9 %convolution_convert_fusion = bf16[512,2048]{1,0:T(8,128)(2,1)} fusion(bf16[512,1024]{1,0:T(8,128)(2,1)S(1)} %copy-done.6, bf16[2048,1024]{1,0:T(8,128)(2,1)} %all-gather.6.cloned.1.call-done), kind=kOutput, calls=%fused_computation.1 | convolution fusion | flops 2148532224 | bytes 7340032 | tf_op jit(solution)/shard_map/dot_general | solution.py:8
  165.1 0.0 reduce-scatter.7.cloned.1.call-update
  165.1 0.2 reduce-scatter.5.cloned.1.call-start
  165.3 16.5 %all-gather.4.cloned.1.call-done = bf16[512,2048]{1,0:T(8,128)(2,1)} async-done(((bf16[128,2048]{1,0:T(8,128)(2,1)}), bf16[512,2048]{1,0:T(8,128)(2,1)}) %all-gather.4.cloned.1.call-update) | async-done | bytes 2097168 | tf_op jit(solution)/shard_map/all_gather | solution.py:22
  181.8 0.0 copy-start.1
  181.8 5.3 convolution_convert_fusion.2
  187.1 0.0 copy-start.4
  187.2 1.0 copy-done.4
  188.1 0.0 copy-done.1
  188.1 3.7 convolution_convert_fusion.1
  191.8 0.0 reduce-scatter.5.cloned.1.call-update
  191.8 1.9 copy.13
  193.7 139.1 %reduce-scatter.11.cloned.1.call-done = f32[128,2048]{1,0:T(8,128)} async-done(((f32[1024,2048]{1,0:T(8,128)}), f32[128,2048]{1,0:T(8,128)}) %reduce-scatter.11.cloned.1.call-update) | async-done | bytes 1048592 | tf_op jit(solution)/shard_map/reduce_scatter | solution.py:59
  332.8 2.6 multiply_add_fusion
  335.5 147.8 %reduce-scatter.9.cloned.1.call-done = f32[256,1024]{0,1:T(8,128)} async-done(((f32[2048,1024]{0,1:T(8,128)}), f32[256,1024]{0,1:T(8,128)}) %reduce-scatter.9.cloned.1.call-update) | async-done | bytes 1048592 | tf_op jit(solution)/shard_map/reduce_scatter | solution.py:54
  483.3 2.3 multiply_add_fusion.1
  485.6 2.5 copy.14
  488.2 28.4 %reduce-scatter.7.cloned.1.call-done = bf16[128,2048]{1,0:T(8,128)(2,1)} async-done(((bf16[512,2048]{1,0:T(8,128)(2,1)}), bf16[128,2048]{1,0:T(8,128)(2,1)}) %reduce-scatter.7.cloned.1.call-update) | async-done | bytes 524304 | tf_op jit(solution)/shard_map/reduce_scatter | solution.py:47
  516.6 34.3 %reduce-scatter.5.cloned.1.call-done = bf16[128,2048]{1,0:T(8,128)(2,1)} async-done(((bf16[512,2048]{1,0:T(8,128)(2,1)}), bf16[128,2048]{1,0:T(8,128)(2,1)}) %reduce-scatter.5.cloned.1.call-update) | async-done | bytes 524304 | tf_op jit(solution)/shard_map/reduce_scatter | solution.py:37
Async XLA Ops:
  7.2 2.3 copy-start
  7.2 78.5 %all-gather.8.cloned.1.call-start = ((), (), s32[]{:S(2)}) async-start(), calls=%async_computation.6 | async-start | bytes 4718592 | tf_op jit(solution)/shard_map/all_gather | solution.py:29
  7.9 151.2 %all-gather.6.cloned.1.call-start = ((), (), s32[]{:S(2)}) async-start(), calls=%async_computation.5 | async-start | bytes 4718592 | tf_op jit(solution)/shard_map/all_gather | solution.py:28
  8.7 173.2 %all-gather.4.cloned.1.call-start = ((), (), s32[]{:S(2)}) async-start(), calls=%async_computation.4 | async-start | bytes 2621440 | tf_op jit(solution)/shard_map/all_gather | solution.py:22
  9.4 323.4 %reduce-scatter.11.cloned.1.call-start = ((), (), s32[]{:S(2)}) async-start(), calls=%async_computation.10 | async-start | bytes 9437184 | tf_op jit(solution)/shard_map/reduce_scatter | solution.py:59
  16.3 69.3 %copy-start.3 = (bf16[512,1024]{1,0:T(8,128)(2,1)S(1)}, bf16[512,1024]{1,0:T(8,128)(2,1)}, u32[]{:S(2)}) copy-start(bf16[512,1024]{1,0:T(8,128)(2,1)} %param.10) | copy-start | bytes 3145732
  16.3 467.0 %reduce-scatter.9.cloned.1.call-start = ((), (), s32[]{:S(2)}) async-start(), calls=%async_computation.9 | async-start | bytes 9437184 | tf_op jit(solution)/shard_map/reduce_scatter | solution.py:54
  85.7 5.7 %copy-start.2 = (bf16[512,2048]{1,0:T(8,128)(2,1)S(1)}, bf16[512,2048]{1,0:T(8,128)(2,1)}, u32[]{:S(2)}) copy-start(bf16[512,2048]{1,0:T(8,128)(2,1)} %param.9) | copy-start | bytes 6291460
  90.4 1.0 copy-start.5
  97.0 62.2 %copy-start.6 = (bf16[512,1024]{1,0:T(8,128)(2,1)S(1)}, bf16[512,1024]{1,0:T(8,128)(2,1)}, u32[]{:S(2)}) copy-start(bf16[512,1024]{1,0:T(8,128)(2,1)} %copy-done.5) | copy-start | bytes 3145732
  97.0 419.6 %reduce-scatter.7.cloned.1.call-start = ((), (), s32[]{:S(2)}) async-start(), calls=%async_computation.8 | async-start | bytes 2621440 | tf_op jit(solution)/shard_map/reduce_scatter | solution.py:47
  165.1 385.8 %reduce-scatter.5.cloned.1.call-start = ((), (), s32[]{:S(2)}) async-start(), calls=%async_computation.7 | async-start | bytes 2621440 | tf_op jit(solution)/shard_map/reduce_scatter | solution.py:37
  181.8 6.3 %copy-start.1 = (bf16[1024,2048]{1,0:T(8,128)(2,1)S(1)}, bf16[1024,2048]{1,0:T(8,128)(2,1)}, u32[]{:S(2)}) copy-start(bf16[1024,2048]{1,0:T(8,128)(2,1)} %all-gather.8.cloned.1.call-done) | copy-start | bytes 12582916
  187.1 1.0 copy-start.4
Sparse Core Ops, SparseCore 0:
  10.1 75.5 all-gather.7
  87.8 71.3 all-gather.5
  160.7 21.0 all-gather.3
  185.3 147.4 reduce-scatter.10
  336.3 146.9 reduce-scatter.8
  486.3 30.2 reduce-scatter.6
  519.7 31.1 reduce-scatter.4
where the time goes:
time: 558 us
  waiting for transfers between devices  500 us (90%)
  matrix products  32.1 us (6%)
  between operations  14.2 us (3%)
  local copies, waits for them, and re-layouts  6.36 us (1%)
    reduce_scatter x1, waiting for transfers between devices, shards(): lax.psum_scatter(contract_first(columns, pre_grad), 'fs', scatter_dimensi...  148 us
    reduce_scatter x1, waiting for transfers between devices, shards(): lax.psum_scatter(contract_first(columns, cotangent), 'fs', scatter_dimens...  139 us
    all_gather x1, waiting for transfers between devices, shards(): lax.all_gather(down_weight, 'fs', axis=0, tiled=True)  69.3 us
    all_gather x1, waiting for transfers between devices, shards(): lax.all_gather(up_weight, 'fs', axis=0, tiled=True)  62.1 us
    reduce_scatter x1, waiting for transfers between devices, shards(): lax.psum_scatter(jnp.dot(rows_here, down_front, preferred_element_type=jn...  34.3 us
    reduce_scatter x1, waiting for transfers between devices, shards(): lax.psum_scatter(contract_last(rows_here, up_back).astype(jnp.bfloat16),...  28.4 us
    all_gather x1, waiting for transfers between devices, shards(): gathered = lax.all_gather(later_input, 'tp', axis=0, tiled=True)  16.5 us
    dot_general x2, matrix products, contract_first(): lax.dot_general(left_rows, right_rows, (((0,), (0,)), ((), ())), preferre...  12.5 us
  transfers between devices with their start and end apart: 7, of which 7 were waited for; matrix products, arithmetic and copies ran while one was open for 7% of the time, Pallas kernels for 0%

commit v1 on v0

--- a/solution.py
+++ b/solution.py
@@ -2,6 +2,19 @@
 import jax.numpy as jnp
 from jax import lax
 from jax.sharding import PartitionSpec as P
+
+
+def collect(x, axis, dim):
+    size, place, rows = (lax.axis_size(axis), lax.axis_index(axis), x.shape[dim])
+    right = [(i, (i + 1) % size) for i in range(size)]
+    out = jnp.zeros((*x.shape[:dim], size * rows, *x.shape[dim + 1 :]), x.dtype)
+    carried = x
+    for step in range(size):
+        holder = (place - step) % size
+        out = lax.dynamic_update_slice_in_dim(out, carried, holder * rows, axis=dim)
+        if step < size - 1:
+            carried = lax.ppermute(carried, axis, right)
+    return out
 
 
 def contract_last(left_rows, right_rows):
@@ -26,7 +39,7 @@
     activation = (lifted * lifted).astype(jnp.bfloat16)
     up_front, down_front = (
         lax.all_gather(up_weight, "fs", axis=0, tiled=True),
-        lax.all_gather(down_weight, "fs", axis=0, tiled=True),
+        collect(down_weight, "fs", 0),
     )
     later_hidden = jnp.dot(gathered, up_front, preferred_element_type=jnp.float32).astype(
         jnp.bfloat16

time: 558 us -> 524 us (0.939)
  waiting for transfers between devices: 500 us -> 460 us
    ppermute x0 -> x7, waiting for transfers between devices: none -> 147 us  [collect(): carried = lax.ppermute(carried, axis, right)]
    all_gather x1 -> x0, waiting for transfers between devices: 69.3 us -> none  [shards(): lax.all_gather(down_weight, 'fs', axis=0, tiled=True)]
    all_gather x1, waiting for transfers between devices: 62.1 us -> 0.02 us  [shards(): lax.all_gather(up_weight, 'fs', axis=0, tiled=True)]
    reduce_scatter x1, waiting for transfers between devices: 139 us -> 101 us  [shards(): lax.psum_scatter(contract_first(columns, cotangent), 'fs', scatter_dimens...]
    all_gather x1, waiting for transfers between devices: 16.5 us -> 0.02 us  [shards(): gathered = lax.all_gather(later_input, 'tp', axis=0, tiled=True)]
    reduce_scatter x1, waiting for transfers between devices: 34.3 us -> 28.3 us  [shards(): lax.psum_scatter(jnp.dot(rows_here, down_front, preferred_element_type=jn...]
    reduce_scatter x1, waiting for transfers between devices: 28.4 us -> 34.2 us  [shards(): lax.psum_scatter(contract_last(rows_here, up_back).astype(jnp.bfloat16),...]
  transfers between devices with their start and end apart: 7 -> 13, of which waited for: 7 -> 11; matrix products, arithmetic and copies ran while one was open for 7% -> 8% of each run, Pallas kernels for 0% -> 0%
where the time goes in v1:
time: 524 us
  waiting for transfers between devices  460 us (88%)
  matrix products  29.9 us (6%)
  between operations  14.3 us (3%)
  local copies, waits for them, and re-layouts  11.4 us (2%)
    reduce_scatter x1, waiting for transfers between devices, shards(): lax.psum_scatter(contract_first(columns, pre_grad), 'fs', scatter_dimensi...  148 us
    ppermute x7, waiting for transfers between devices, collect(): carried = lax.ppermute(carried, axis, right)  147 us
    reduce_scatter x1, waiting for transfers between devices, shards(): lax.psum_scatter(contract_first(columns, cotangent), 'fs', scatter_dimens...  101 us
    reduce_scatter x1, waiting for transfers between devices, shards(): lax.psum_scatter(contract_last(rows_here, up_back).astype(jnp.bfloat16),...  34.2 us
    reduce_scatter x1, waiting for transfers between devices, shards(): lax.psum_scatter(jnp.dot(rows_here, down_front, preferred_element_type=jn...  28.3 us
    dot_general x2, matrix products, contract_first(): lax.dot_general(left_rows, right_rows, (((0,), (0,)), ((), ())), preferre...  12.5 us
  transfers between devices with their start and end apart: 13, of which 11 were waited for; matrix products, arithmetic and copies ran while one was open for 8% of the time, Pallas kernels for 0%

profile of v1, /device:TPU:0, one launch (start us, length us, event | category | flops | bytes accessed | tf_op | source)
XLA Modules:
  0.0 523.6 jit_solution(11652913300027718504)
XLA Ops:
  7.2 0.0 all-gather.3.cloned.1.call-start
  7.2 0.7 all-gather.3.cloned.1.call-update
  7.9 0.0 all-gather.5.cloned.1.call-start
  8.0 0.7 all-gather.5.cloned.1.call-update
  8.7 0.0 reduce-scatter.11.cloned.1.call-start
  8.7 0.1 copy-done
  8.8 6.9 %fusion.1 = f32[1024,2048]{1,0:T(8,128)} fusion(bf16[512,2048]{1,0:T(8,128)(2,1)S(1)} %copy-done, bf16[512,1024]{1,0:T(8,128)(2,1)} %param.10), kind=kOutput, calls=%fused_computation.9 | convolution fusion | flops 2149580800 | bytes 11534336 | tf_op jit(solution)/shard_map/dot_general | solution.py:27
  15.6 0.0 reduce-scatter.11.cloned.1.call-update
  15.7 0.0 reduce-scatter.9.cloned.1.call-start
  15.7 1.0 copy-done.3
  16.7 3.0 collective-permute-start
  19.7 15.0 %collective-permute-done = bf16[128,2048]{1,0:T(8,128)(2,1)S(1)} collective-permute-done((bf16[128,2048]{1,0:T(8,128)(2,1)S(1)}, bf16[128,2048]{1,0:T(8,128)(2,1)S(1)}, u32[]{:S(2)}, u32[]{:S(2)}) %collective-permute-start) | collective-permute-done | bytes 524320 | tf_op jit(solution)/shard_map/ppermute | solution.py:16
  34.6 15.9 %collective-permute-done.1 = bf16[128,2048]{1,0:T(8,128)(2,1)S(1)} collective-permute-done((bf16[128,2048]{1,0:T(8,128)(2,1)S(1)}, bf16[128,2048]{1,0:T(8,128)(2,1)S(1)}, u32[]{:S(2)}, u32[]{:S(2)}) %collective-permute-start.1) | collective-permute-done | bytes 524320 | tf_op jit(solution)/shard_map/ppermute | solution.py:16
  50.5 0.8 copy-done.4
  51.3 27.6 %collective-permute-done.2 = bf16[128,2048]{1,0:T(8,128)(2,1)S(1)} collective-permute-done((bf16[128,2048]{1,0:T(8,128)(2,1)S(1)}, bf16[128,2048]{1,0:T(8,128)(2,1)S(1)}, u32[]{:S(2)}, u32[]{:S(2)}) %collective-permute-start.2) | collective-permute-done | bytes 524320 | tf_op jit(solution)/shard_map/ppermute | solution.py:16
  78.9 0.8 copy-done.6
  79.7 26.2 %collective-permute-done.3 = bf16[128,2048]{1,0:T(8,128)(2,1)} collective-permute-done((bf16[128,2048]{1,0:T(8,128)(2,1)S(1)}, bf16[128,2048]{1,0:T(8,128)(2,1)}, u32[]{:S(2)}, u32[]{:S(2)}) %collective-permute-start.3) | collective-permute-done | bytes 524320 | tf_op jit(solution)/shard_map/ppermute | solution.py:16
  105.9 0.5 broadcast_in_dim.3
  106.5 0.1 constant_dynamic-update-slice_fusion.7
  106.5 26.5 %collective-permute-done.4 = bf16[128,2048]{1,0:T(8,128)(2,1)} collective-permute-done((bf16[128,2048]{1,0:T(8,128)(2,1)}, bf16[128,2048]{1,0:T(8,128)(2,1)}, u32[]{:S(2)}, u32[]{:S(2)}) %collective-permute-start.4) | collective-permute-done | bytes 524320 | tf_op jit(solution)/shard_map/ppermute | solution.py:16
  133.1 0.1 constant_dynamic-update-slice_fusion.5
  133.2 0.1 constant_dynamic-update-slice_fusion.4
  133.3 17.0 %collective-permute-done.5 = bf16[128,2048]{1,0:T(8,128)(2,1)S(1)} collective-permute-done((bf16[128,2048]{1,0:T(8,128)(2,1)}, bf16[128,2048]{1,0:T(8,128)(2,1)S(1)}, u32[]{:S(2)}, u32[]{:S(2)}) %collective-permute-start.5) | collective-permute-done | bytes 524320 | tf_op jit(solution)/shard_map/ppermute | solution.py:16
  150.3 1.1 constant_dynamic-update-slice_fusion.3
  151.4 1.1 constant_dynamic-update-slice_fusion.2
  152.5 18.4 %collective-permute-done.6 = bf16[128,2048]{1,0:T(8,128)(2,1)S(1)} collective-permute-done((bf16[128,2048]{1,0:T(8,128)(2,1)S(1)}, bf16[128,2048]{1,0:T(8,128)(2,1)S(1)}, u32[]{:S(2)}, u32[]{:S(2)}) %collective-permute-start.6) | collective-permute-done | bytes 524320 | tf_op jit(solution)/shard_map/ppermute | solution.py:16
  171.0 2.4 fusion
  173.4 0.7 copy-done.8
  174.1 5.6 %convolution_bitcast_fusion = f32[2048,1024]{0,1:T(8,128)} fusion(bf16[512,1024]{1,0:T(8,128)(2,1)S(1)} %fusion, bf16[512,2048]{1,0:T(8,128)(2,1)S(1)} %copy-done.8), kind=kOutput, calls=%fused_computation | convolution fusion | flops 2147483648 | bytes 11534336 | tf_op jit(solution)/shard_map/dot_general | solution.py:27
  179.7 0.0 reduce-scatter.9.cloned.1.call-update
  179.7 0.0 reduce-scatter.5.cloned.1.call-start
  179.8 0.0 all-gather.3.cloned.1.call-done
  179.8 0.0 all-gather.5.cloned.1.call-done
  179.9 5.3 %convolution_convert_fusion.2 = bf16[512,1024]{1,0:T(8,128)(2,1)S(1)} fusion(bf16[512,2048]{1,0:T(8,128)(2,1)} %all-gather.3.cloned.1.call-done, bf16[2048,1024]{1,0:T(8,128)(2,1)} %all-gather.5.cloned.1.call-done), kind=kOutput, calls=%fused_computation.8 | convolution fusion | flops 2148007936 | bytes 7340032 | tf_op jit(solution)/shard_map/dot_general | solution.py:44
  185.2 1.0 copy-done.10
  186.2 3.7 convolution_convert_fusion.1
  189.9 0.0 reduce-scatter.5.cloned.1.call-update
  189.9 0.2 reduce-scatter.7.cloned.1.call-start
  190.1 6.0 %convolution_convert_fusion = bf16[512,2048]{1,0:T(8,128)(2,1)} fusion(bf16[512,1024]{1,0:T(8,128)(2,1)S(1)} %fusion, bf16[2048,1024]{1,0:T(8,128)(2,1)} %all-gather.5.cloned.1.call-done), kind=kOutput, calls=%fused_computation.1 | convolution fusion | flops 2148532224 | bytes 7340032 | tf_op jit(solution)/shard_map/dot_general | solution.py:21
  196.1 0.0 reduce-scatter.7.cloned.1.call-update
  196.1 1.6 copy.14
  197.7 101.2 %reduce-scatter.11.cloned.1.call-done = f32[128,2048]{1,0:T(8,128)} async-done(((f32[1024,2048]{1,0:T(8,128)}), f32[128,2048]{1,0:T(8,128)}) %reduce-scatter.11.cloned.1.call-update) | async-done | bytes 1048592 | tf_op jit(solution)/shard_map/reduce_scatter | solution.py:72
  298.9 2.6 multiply_add_fusion
  301.5 147.8 %reduce-scatter.9.cloned.1.call-done = f32[256,1024]{0,1:T(8,128)} async-done(((f32[2048,1024]{0,1:T(8,128)}), f32[256,1024]{0,1:T(8,128)}) %reduce-scatter.9.cloned.1.call-update) | async-done | bytes 1048592 | tf_op jit(solution)/shard_map/reduce_scatter | solution.py:67
  449.4 2.4 multiply_add_fusion.1
  451.8 2.5 copy.15
  454.3 28.3 %reduce-scatter.5.cloned.1.call-done = bf16[128,2048]{1,0:T(8,128)(2,1)} async-done(((bf16[512,2048]{1,0:T(8,128)(2,1)}), bf16[128,2048]{1,0:T(8,128)(2,1)}) %reduce-scatter.5.cloned.1.call-update) | async-done | bytes 524304 | tf_op jit(solution)/shard_map/reduce_scatter | solution.py:50
  482.6 34.2 %reduce-scatter.7.cloned.1.call-done = bf16[128,2048]{1,0:T(8,128)(2,1)} async-done(((bf16[512,2048]{1,0:T(8,128)(2,1)}), bf16[128,2048]{1,0:T(8,128)(2,1)}) %reduce-scatter.7.cloned.1.call-update) | async-done | bytes 524304 | tf_op jit(solution)/shard_map/reduce_scatter | solution.py:60
  (25 shorter events, 0.2 us)
Async XLA Ops:
  7.2 1.6 copy-start
  7.2 172.6 %all-gather.3.cloned.1.call-start = ((), (), s32[]{:S(2)}) async-start(), calls=%async_computation.4 | async-start | bytes 2621440 | tf_op jit(solution)/shard_map/all_gather | solution.py:35
  7.9 171.9 %all-gather.5.cloned.1.call-start = ((), (), s32[]{:S(2)}) async-start(), calls=%async_computation.5 | async-start | bytes 4718592 | tf_op jit(solution)/shard_map/all_gather | solution.py:41
  8.7 290.2 %reduce-scatter.11.cloned.1.call-start = ((), (), s32[]{:S(2)}) async-start(), calls=%async_computation.9 | async-start | bytes 9437184 | tf_op jit(solution)/shard_map/reduce_scatter | solution.py:72
  15.6 1.0 copy-start.3
  15.7 433.7 %reduce-scatter.9.cloned.1.call-start = ((), (), s32[]{:S(2)}) async-start(), calls=%async_computation.8 | async-start | bytes 9437184 | tf_op jit(solution)/shard_map/reduce_scatter | solution.py:67
  16.7 18.0 %collective-permute-start = (bf16[128,2048]{1,0:T(8,128)(2,1)S(1)}, bf16[128,2048]{1,0:T(8,128)(2,1)S(1)}, u32[]{:S(2)}, u32[]{:S(2)}) collective-permute-start(bf16[128,2048]{1,0:T(8,128)(2,1)S(1)} %copy-done.3), channel_id=1, source_target_pairs={{0,4},{4,8},{8,12},{12,16},{16,20},{20,24},{24,28},{28,0},{1,5},{5... | collective-permute-start | bytes 1572872 | tf_op jit(solution)/shard_map/ppermute | solution.py:16
  34.6 15.9 %collective-permute-start.1 = (bf16[128,2048]{1,0:T(8,128)(2,1)S(1)}, bf16[128,2048]{1,0:T(8,128)(2,1)S(1)}, u32[]{:S(2)}, u32[]{:S(2)}) collective-permute-start(bf16[128,2048]{1,0:T(8,128)(2,1)S(1)} %collective-permute-done), channel_id=1, source_target_pairs={{0,4},{4,8},{8,12},{12,16},{16,20},{20,24},{24,28},{28,0},{1,5},{5... | collective-permute-start | bytes 1572872 | tf_op jit(solution)/shard_map/ppermute | solution.py:16
  50.5 0.8 copy-start.4
  51.3 27.6 %collective-permute-start.2 = (bf16[128,2048]{1,0:T(8,128)(2,1)S(1)}, bf16[128,2048]{1,0:T(8,128)(2,1)S(1)}, u32[]{:S(2)}, u32[]{:S(2)}) collective-permute-start(bf16[128,2048]{1,0:T(8,128)(2,1)S(1)} %collective-permute-done.1), channel_id=1, source_target_pairs={{0,4},{4,8},{8,12},{12,16},{16,20},{20,24},{24,28},{28,0},{1,5},{5... | collective-permute-start | bytes 1572872 | tf_op jit(solution)/shard_map/ppermute | solution.py:16
  78.9 0.8 copy-start.6
  79.7 26.2 %collective-permute-start.3 = (bf16[128,2048]{1,0:T(8,128)(2,1)S(1)}, bf16[128,2048]{1,0:T(8,128)(2,1)}, u32[]{:S(2)}, u32[]{:S(2)}) collective-permute-start(bf16[128,2048]{1,0:T(8,128)(2,1)S(1)} %collective-permute-done.2), channel_id=1, source_target_pairs={{0,4},{4,8},{8,12},{12,16},{16,20},{20,24},{24,28},{28,0},{1,5},{5... | collective-permute-start | bytes 1572872 | tf_op jit(solution)/shard_map/ppermute | solution.py:16
  105.9 27.1 %collective-permute-start.4 = (bf16[128,2048]{1,0:T(8,128)(2,1)}, bf16[128,2048]{1,0:T(8,128)(2,1)}, u32[]{:S(2)}, u32[]{:S(2)}) collective-permute-start(bf16[128,2048]{1,0:T(8,128)(2,1)} %collective-permute-done.3), channel_id=1, source_target_pairs={{0,4},{4,8},{8,12},{12,16},{16,20},{20,24},{24,28},{28,0},{1,5},{5... | collective-permute-start | bytes 1572872 | tf_op jit(solution)/shard_map/ppermute | solution.py:16
  105.9 27.2 %copy-start.5 = (bf16[128,2048]{1,0:T(8,128)(2,1)S(1)}, bf16[128,2048]{1,0:T(8,128)(2,1)}, u32[]{:S(2)}) copy-start(bf16[128,2048]{1,0:T(8,128)(2,1)} %copy-done.4) | copy-start | bytes 1572868
  105.9 27.3 %copy-start.7 = (bf16[128,2048]{1,0:T(8,128)(2,1)S(1)}, bf16[128,2048]{1,0:T(8,128)(2,1)}, u32[]{:S(2)}) copy-start(bf16[128,2048]{1,0:T(8,128)(2,1)} %copy-done.6) | copy-start | bytes 1572868
  106.4 64.5 %copy-start.9 = (bf16[512,1024]{1,0:T(8,128)(2,1)S(1)}, bf16[512,1024]{1,0:T(8,128)(2,1)}, u32[]{:S(2)}) copy-start(bf16[512,1024]{1,0:T(8,128)(2,1)} %param.10) | copy-start | bytes 3145732
  133.1 17.2 %collective-permute-start.5 = (bf16[128,2048]{1,0:T(8,128)(2,1)}, bf16[128,2048]{1,0:T(8,128)(2,1)S(1)}, u32[]{:S(2)}, u32[]{:S(2)}) collective-permute-start(bf16[128,2048]{1,0:T(8,128)(2,1)} %collective-permute-done.4), channel_id=1, source_target_pairs={{0,4},{4,8},{8,12},{12,16},{16,20},{20,24},{24,28},{28,0},{1,5},{5... | collective-permute-start | bytes 1572872 | tf_op jit(solution)/shard_map/ppermute | solution.py:16
  150.3 20.6 %collective-permute-start.6 = (bf16[128,2048]{1,0:T(8,128)(2,1)S(1)}, bf16[128,2048]{1,0:T(8,128)(2,1)S(1)}, u32[]{:S(2)}, u32[]{:S(2)}) collective-permute-start(bf16[128,2048]{1,0:T(8,128)(2,1)S(1)} %collective-permute-done.5), channel_id=1, source_target_pairs={{0,4},{4,8},{8,12},{12,16},{16,20},{20,24},{24,28},{28,0},{1,5},{5... | collective-permute-start | bytes 1572872 | tf_op jit(solution)/shard_map/ppermute | solution.py:16
  171.0 2.4 copy-start.1
  171.0 3.1 copy-start.8
  179.7 302.8 %reduce-scatter.5.cloned.1.call-start = ((), (), s32[]{:S(2)}) async-start(), calls=%async_computation.6 | async-start | bytes 2621440 | tf_op jit(solution)/shard_map/reduce_scatter | solution.py:50
  179.8 6.3 %copy-start.2 = (bf16[1024,2048]{1,0:T(8,128)(2,1)S(1)}, bf16[1024,2048]{1,0:T(8,128)(2,1)}, u32[]{:S(2)}) copy-start(bf16[1024,2048]{1,0:T(8,128)(2,1)} %copy-done.1) | copy-start | bytes 12582916
  185.2 1.0 copy-start.10
  189.9 326.8 %reduce-scatter.7.cloned.1.call-start = ((), (), s32[]{:S(2)}) async-start(), calls=%async_computation.7 | async-start | bytes 2621440 | tf_op jit(solution)/shard_map/reduce_scatter | solution.py:60
Sparse Core Ops, SparseCore 0:
  9.5 25.2 all-gather.2
  37.0 101.0 all-gather.4
  141.7 157.1 reduce-scatter.10
  302.4 146.9 reduce-scatter.8
  452.3 30.2 reduce-scatter.4
  485.5 31.1 reduce-scatter.6
